TPU v7x, 32 devices: a whole 2x2x4 slice. The times are simulated.
32 devices in a mesh: ep: 8 (over z, y), tp: 4 (over x, core).
Axes of the slice: x: 2, y: 2, z: 4, core: 2. Of those that a mesh axis runs over, the one named last changes fastest.
Arguments:
- outer_gate: bfloat16 [4096, 2048], P('ep', 'tp'), may hold values from -6 to 6
- inner_gate: bfloat16 [4096, 2048], P('ep', 'tp'), may hold values from -6 to 6
- conv_values: bfloat16 [4096, 2048], P('ep', 'tp'), may hold values from -6 to 6
- conv_taps: bfloat16 [3, 2048], P(None, 'tp'), may hold values from -3 to 3
- out_weight: bfloat16 [2048, 2048], P('tp'), may hold values from -0.125 to 0.125
- moe_input: bfloat16 [4096, 2048], P(('ep', 'tp')), may hold values from -6 to 6
- norm_gain: bfloat16 [2048], replicated, may hold values from 0.099609375 to 1.8984375
- gate_proj: bfloat16 [8, 2048, 1024], P('ep', None, 'tp'), may hold values from -0.125 to 0.125
- up_proj: bfloat16 [8, 2048, 1024], P('ep', None, 'tp'), may hold values from -0.125 to 0.125
- down_proj: bfloat16 [8, 1024, 2048], P('ep', 'tp'), may hold values from -0.1875 to 0.1875
- shared_gate: bfloat16 [2048, 1024], P(None, 'tp'), may hold values from -0.125 to 0.125
- shared_up: bfloat16 [2048, 1024], P(None, 'tp'), may hold values from -0.125 to 0.125
- shared_down: bfloat16 [1024, 2048], P('tp'), may hold values from -0.1875 to 0.1875
- routes: int32 [4096, 2], P('ep'), may hold values from 0 to 7, all different within a row; in each aligned block of 128 rows (0 to 127, 128 to 255, ...) at most 64 rows name the same one
- route_weight: float32 [4096, 2], P('ep'), may hold values from 0.3 to 1.5
Outputs:
- mixer_out: bfloat16 [4096, 2048], P(('ep', 'tp'))
- expert_mix: bfloat16 [4096, 2048], P(('ep', 'tp'))
Inputs may be any that keep to these rules, and one draw needn't show every extreme that they name: `routes`: each row names 2 different experts. In the 128 rows of one device no expert is named more than 64 times, and in every draw some expert is named exactly 64 times in one device's rows.
All inputs are finite; a program needn't handle non-finite values.
Results may differ from a plain program's by a relative error of at most 0.012.
Values may be sent and summed in bfloat16 or wider, within the bound.
A program may use at most 128 MiB of HBM per device.

v0:
```python
from functools import partial
import jax
import jax.numpy as jnp
from jax import lax
from jax.sharding import PartitionSpec as P

epsilon = 1e-06


def shifted(block, axis, distance):
    devices = range(lax.axis_size(axis))
    route = [(i - distance, i) for i in devices if i - distance in devices]
    return lax.ppermute(block, axis, route)


def rms_norm(inputs, scales):
    values = inputs.astype(jnp.float32)
    square = jnp.mean(values * values, axis=-1, keepdims=True)
    return (values * lax.rsqrt(square + epsilon) * scales.astype(jnp.float32)).astype(jnp.bfloat16)


def swiglu(inputs, gate_w, up_w):
    gate_term = jnp.dot(inputs, gate_w, preferred_element_type=jnp.float32)
    upward = jnp.dot(inputs, up_w, preferred_element_type=jnp.float32)
    return (jax.nn.silu(gate_term) * upward).astype(jnp.bfloat16)


def slot_table(block_routes, experts, capacity):
    flat_ids = block_routes.reshape(-1)
    onehot = (flat_ids[:, None] == jnp.arange(experts, dtype=jnp.int32)[None, :]).astype(jnp.int32)
    earlier = jnp.cumsum(onehot, axis=0) - onehot
    slot_ids = jnp.sum(earlier * onehot, axis=1)
    targets = flat_ids * capacity + slot_ids
    owners = jnp.arange(flat_ids.shape[0], dtype=jnp.int32) // block_routes.shape[1]
    sources = jnp.zeros((experts * capacity,), jnp.int32).at[targets].set(owners)
    filled = jnp.zeros((experts * capacity,), jnp.bfloat16).at[targets].set(1.0)
    return (sources, filled, targets)


def send_own(normed, own_routes, table_maker, ep_count, capacity):
    sources, filled, own_targets = table_maker(own_routes)
    outgoing = (normed[sources] * filled[:, None]).reshape(ep_count, capacity, normed.shape[1])
    landed = lax.all_to_all(outgoing, "ep", split_axis=0, concat_axis=0, tiled=True)
    return (landed, own_targets)


def per_device(
    outer_gate,
    inner_gate,
    conv_values,
    conv_taps,
    out_weight,
    moe_input,
    norm_gain,
    gate_proj,
    up_proj,
    down_proj,
    shared_gate,
    shared_up,
    shared_down,
    routes,
    route_weight,
):
    tp_count = lax.axis_size("tp")
    ep_count = lax.axis_size("ep")
    my_slot = lax.axis_index("tp")
    group_len = inner_gate.shape[0]
    mix_rows = group_len // tp_count
    channels = inner_gate.shape[1]
    model_width = moe_input.shape[1]
    own_rows = moe_input.shape[0]
    top_count = routes.shape[1]
    capacity = 2 * own_rows * top_count // ep_count
    slot_rows = ep_count * capacity
    reach_rows = conv_taps.shape[0] - 1
    edge_rows = jnp.stack(
        (inner_gate[group_len - reach_rows :], conv_values[group_len - reach_rows :])
    )
    before = shifted(edge_rows, "ep", 1)
    full_gate = jnp.concatenate((before[0], inner_gate), axis=0).astype(jnp.float32)
    full_values = jnp.concatenate((before[1], conv_values), axis=0).astype(jnp.float32)
    product = full_gate * full_values
    tap_values = conv_taps.astype(jnp.float32)
    convolved = tap_values[0] * product[0:group_len]
    for offset in range(1, reach_rows + 1):
        convolved = convolved + tap_values[offset] * product[offset : offset + group_len]
    gate_rows = (outer_gate.astype(jnp.float32) * convolved).astype(jnp.bfloat16)
    gate_rows = gate_rows.reshape(tp_count, mix_rows, channels)
    normed = rms_norm(moe_input, norm_gain)
    group_normed = lax.all_gather(normed, "tp", axis=0, tiled=True)
    group_split = group_normed.reshape(tp_count, own_rows, model_width)
    own_weights = lax.dynamic_slice_in_dim(route_weight, my_slot * own_rows, own_rows, 0)
    own_routes = lax.dynamic_slice_in_dim(routes, my_slot * own_rows, own_rows, 0)
    table_maker = partial(slot_table, experts=ep_count, capacity=capacity)
    local_routed = None
    landed, own_targets = send_own(normed, own_routes, table_maker, ep_count, capacity)
    gate_full, up_full, down_full = (
        lax.all_gather(gate_proj, "tp", axis=2, tiled=True),
        lax.all_gather(up_proj, "tp", axis=2, tiled=True),
        lax.all_gather(down_proj, "tp", axis=1, tiled=True),
    )
    hidden = swiglu(landed.reshape(slot_rows, model_width), gate_full[0], up_full[0])
    unit_block = hidden.shape[1] // tp_count
    local_routed = jnp.zeros((slot_rows, model_width), jnp.float32)
    for piece_idx in range(tp_count):
        partial_sum = jnp.dot(
            hidden[:, piece_idx * unit_block : (piece_idx + 1) * unit_block],
            down_full[0, piece_idx * unit_block : (piece_idx + 1) * unit_block],
            preferred_element_type=jnp.float32,
        ).astype(jnp.bfloat16)
        local_routed = local_routed + partial_sum.astype(jnp.float32)
    routed_rows = 0
    expert_block = routed_rows + own_rows
    joint_block = mix_rows + expert_block
    dev_count = joint_block * lax.axis_size("tp") // joint_block
    block_rows = gate_rows
    block_rows = block_rows.reshape(dev_count * mix_rows, channels)
    projected = jnp.dot(block_rows, out_weight, preferred_element_type=jnp.float32)
    shared_in = group_split
    shared_in = shared_in.reshape(dev_count * own_rows, model_width)
    shared_out = jnp.dot(
        swiglu(shared_in, shared_gate, shared_up), shared_down, preferred_element_type=jnp.float32
    )
    shared_out = shared_out.reshape(dev_count, own_rows, model_width)
    combined = jnp.concatenate(
        (projected.reshape(dev_count, mix_rows, model_width), shared_out), axis=1
    )
    summed = lax.psum_scatter(
        combined.reshape(dev_count * joint_block, model_width).astype(jnp.bfloat16),
        "tp",
        scatter_dimension=0,
        tiled=True,
    ).astype(jnp.float32)
    mixer_out = summed[:mix_rows].astype(jnp.bfloat16)
    expert_total = summed[mix_rows:]
    routed_back = local_routed.astype(jnp.bfloat16)
    routed_back = routed_back.reshape(ep_count, capacity, model_width)
    returned = lax.all_to_all(routed_back, "ep", split_axis=0, concat_axis=0, tiled=True).reshape(
        slot_rows, model_width
    )
    picked = returned[own_targets].reshape(own_rows, top_count, model_width).astype(jnp.float32)
    routed = jnp.sum(picked * own_weights[:, :, None], axis=1)
    expert_mix = (expert_total + routed).astype(jnp.bfloat16)
    return (mixer_out, expert_mix)


def solution(mesh):
    return jax.shard_map(
        per_device,
        mesh=mesh,
        in_specs=(
            P("ep", "tp"),
            P("ep", "tp"),
            P("ep", "tp"),
            P(None, "tp"),
            P("tp", None),
            P(("ep", "tp"), None),
            P(),
            P("ep", None, "tp"),
            P("ep", None, "tp"),
            P("ep", "tp", None),
            P(None, "tp"),
            P(None, "tp"),
            P("tp", None),
            P("ep", None),
            P("ep", None),
        ),
        out_specs=(P(("ep", "tp"), None), P(("ep", "tp"), None)),
        check_vma=False,
    )
```

profile of v0, /device:TPU:0, one launch (start us, length us, event | category | flops | bytes accessed | tf_op | source)
XLA Modules:
  0.0 229.2 jit_solution(8211461132235295244)
XLA Ops:
  9.3 2.0 fusion.9
  17.2 3.3 %gather_fusion = bf16[512,2048]{1,0:T(8,128)(2,1)} fusion(bf16[128,2048]{1,0:T(8,128)(2,1)S(1)} %copy-done.1, s32[1024]{0:T(1024)S(1)} %pad_clamp_fusion.1), kind=kCustom, calls=%fused_computation | custom fusion | bytes 4196352 | tf_op jit(solution)/shard_map/gather | solution.py:42
  20.5 2.2 scatter_custom_fusion.1
  22.7 3.1 %broadcast_multiply_fusion = bf16[8,64,2048]{2,1,0:T(8,128)(2,1)} fusion(bf16[8,64,2048]{2,1,0:T(8,128)(2,1)} %bitcast.58, bf16[8,64]{1,0:T(8,128)(2,1)S(1)} %mul.134), kind=kLoop, calls=%fused_computation.38 | loop fusion | flops 1048576 | bytes 4195328 | tf_op jit(solution)/shard_map/mul | solution.py:42
  25.8 7.4 %all-to-all-start = ((bf16[8,64,2048]{2,1,0:T(8,128)(2,1)}), bf16[8,64,2048]{2,1,0:T(8,128)(2,1)}, u32[]{:S(2)}, u32[]{:S(2)}) async-start(bf16[8,64,2048]{2,1,0:T(8,128)(2,1)} %broadcast_multiply_fusion), calls=%async_computation.1 | async-start | bytes 4194304 | tf_op jit(solution)/shard_map/all_to_all | solution.py:43
  33.4 4.2 %collective-permute-start = (bf16[2,2,512]{2,1,0:T(2,128)(2,1)S(1)}, bf16[2,2,512]{2,1,0:T(2,128)(2,1)S(1)}, u32[]{:S(2)}, u32[]{:S(2)}) collective-permute-start(bf16[2,2,512]{2,1,0:T(2,128)(2,1)S(1)} %pad_maximum_fusion.1), channel_id=1, source_target_pairs={{0,4},{4,8},{8,12},{12,16},{16,20},{20,24},{24,28},{1,5},{5,9},{9,... | collective-permute-start | bytes 12296 | tf_op jit(solution)/shard_map/ppermute | solution.py:13
  37.6 12.8 %collective-permute-done = bf16[2,2,512]{2,1,0:T(2,128)(2,1)S(1)} collective-permute-done((bf16[2,2,512]{2,1,0:T(2,128)(2,1)S(1)}, bf16[2,2,512]{2,1,0:T(2,128)(2,1)S(1)}, u32[]{:S(2)}, u32[]{:S(2)}) %collective-permute-start) | collective-permute-done | bytes 4128 | tf_op jit(solution)/shard_map/ppermute | solution.py:13
  50.7 2.8 %convolution_convert_fusion.5 = bf16[512,2048]{1,0:T(8,128)(2,1)} fusion(bf16[512,2048]{1,0:T(8,128)(2,1)S(1)} %copy-done, f32[514,512]{1,0:T(8,128)S(1)} %convert_multiply_fusion.2, bf16[512,512]{1,0:T(8,128)(2,1)S(1)} %copy-done.7, f32[512]{0:T(512)S(1)} %bitcast.67, f32[512]{0:T(512)S(1)} %bitcast.66, f32[512]{0:T(512)S(1)} %bitcast.65), kind=kOutput, calls=%fused_computation.15 | convolution fusion | flops 1076887552 | bytes 7870464 | tf_op jit(solution)/shard_map/dot_general | solution.py:118
  53.5 3.1 %fusion.37 = f32[512,256]{1,0:T(8,128)} fusion(bf16[512,2048]{1,0:T(8,128)(2,1)} %all-gather.5.cloned.1.call-done, bf16[2048,256]{1,0:T(8,128)(2,1)S(1)} %copy-done.6), kind=kOutput, calls=%fused_computation.82 | convolution fusion | flops 536870912 | bytes 3670016 | tf_op jit(solution)/shard_map/dot_general | solution.py:23
  56.6 6.0 %convolution_convert_fusion.4 = bf16[512,2048]{1,0:T(8,128)(2,1)} fusion(bf16[256,2048]{1,0:T(8,128)(2,1)} %param.27, bf16[512,2048]{1,0:T(8,128)(2,1)} %all-gather.5.cloned.1.call-done, bf16[2048,256]{1,0:T(8,128)(2,1)} %param.26, f32[512,256]{1,0:T(8,128)} %fusion.37), kind=kOutput, calls=%fused_computation.14 | convolution fusion | flops 1075576832 | bytes 6815744 | tf_op jit(solution)/shard_map/dot_general | solution.py:121
  62.6 4.8 %pad_maximum_fusion = bf16[4,256,2048]{2,1,0:T(8,128)(2,1)} fusion(bf16[4,128,2048]{2,1,0:T(8,128)(2,1)} %bitcast.60, bf16[4,128,2048]{2,1,0:T(8,128)(2,1)} %bitcast.59), kind=kLoop, calls=%fused_computation.4 | loop fusion | flops 8388608 | bytes 8388608 | tf_op jit(solution)/shard_map/concatenate | solution.py:125
  67.4 14.2 %all-to-all-done = bf16[8,64,2048]{2,1,0:T(8,128)(2,1)} async-done(((bf16[8,64,2048]{2,1,0:T(8,128)(2,1)}), bf16[8,64,2048]{2,1,0:T(8,128)(2,1)}, u32[]{:S(2)}, u32[]{:S(2)}) %all-to-all-start) | async-done | bytes 2097184 | tf_op jit(solution)/shard_map/all_to_all | solution.py:43
  81.6 7.2 %fusion.2 = f32[512,1024]{1,0:T(8,128)} fusion(bf16[512,2048]{1,0:T(8,128)(2,1)} %bitcast.15, bf16[1,2048,1024]{2,1,0:T(8,128)(2,1)} %all-gather.7.cloned.1.call-done), kind=kOutput, calls=%fused_computation.7 | convolution fusion | flops 2147483648 | bytes 8388608 | tf_op jit(solution)/shard_map/dot_general | solution.py:23
  88.8 21.2 %all-gather.9.cloned.1.call-done = bf16[1,2048,1024]{2,1,0:T(8,128)(2,1)} async-done(((bf16[1,2048,256]{2,1,0:T(8,128)(2,1)}), bf16[1,2048,1024]{2,1,0:T(8,128)(2,1)}) %all-gather.9.cloned.1.call-update) | async-done | bytes 4194320 | tf_op jit(solution)/shard_map/all_gather | solution.py:99
  110.0 5.9 %multiply_convert_fusion = bf16[512,1024]{1,0:T(8,128)(2,1)S(1)} fusion(f32[512,1024]{1,0:T(8,128)} %fusion.2, bf16[512,2048]{1,0:T(8,128)(2,1)} %bitcast.15, bf16[1,2048,1024]{2,1,0:T(8,128)(2,1)} %all-gather.9.cloned.1.call-done), kind=kOutput, calls=%fused_computation.17 | convolution fusion | flops 2150629376 | bytes 9437184 | tf_op jit(solution)/shard_map/dot_general | solution.py:24
  115.9 30.0 %all-gather.11.cloned.1.call-done = bf16[1,1024,2048]{2,1,0:T(8,128)(2,1)} async-done(((bf16[1,256,2048]{2,1,0:T(8,128)(2,1)}), bf16[1,1024,2048]{2,1,0:T(8,128)(2,1)}) %all-gather.11.cloned.1.call-update) | async-done | bytes 4194320 | tf_op jit(solution)/shard_map/all_gather | solution.py:100
  145.9 2.1 convolution_convert_fusion
  150.6 2.6 %add_convert_fusion = bf16[512,2048]{1,0:T(8,128)(2,1)} fusion(bf16[512,2048]{1,0:T(8,128)(2,1)S(1)} %convolution_convert_fusion, bf16[512,2048]{1,0:T(8,128)(2,1)S(1)} %convolution_convert_fusion.1, bf16[512,2048]{1,0:T(8,128)(2,1)S(1)} %convolution_convert_fusion.2, bf16[1,1024,2048]{2,1,0:T(8,128)(2,1)S(1)} %copy-done.2, ...), kind=kOutput, calls=%fused_computation.9 | convolution fusion | flops 546308096 | bytes 9699328 | tf_op jit(solution)/shard_map/dot_general | solution.py:106
  153.2 5.5 %all-to-all-start.1 = ((bf16[8,64,2048]{2,1,0:T(8,128)(2,1)}), bf16[8,64,2048]{2,1,0:T(8,128)(2,1)}, u32[]{:S(2)}, u32[]{:S(2)}) async-start(bf16[8,64,2048]{2,1,0:T(8,128)(2,1)} %bitcast.57), calls=%async_computation.2 | async-start | bytes 4194304 | tf_op jit(solution)/shard_map/all_to_all | solution.py:138
  159.5 47.9 %all-to-all-done.1 = bf16[8,64,2048]{2,1,0:T(8,128)(2,1)} async-done(((bf16[8,64,2048]{2,1,0:T(8,128)(2,1)}), bf16[8,64,2048]{2,1,0:T(8,128)(2,1)}, u32[]{:S(2)}, u32[]{:S(2)}) %all-to-all-start.1) | async-done | bytes 2097184 | tf_op jit(solution)/shard_map/all_to_all | solution.py:138
  207.5 4.2 %gather_fusion.1 = bf16[256,2048]{1,0:T(8,128)(2,1)S(1)} fusion(bf16[512,2048]{1,0:T(8,128)(2,1)} %bitcast.23, s32[1024]{0:T(1024)S(1)} %pad_clamp_fusion), kind=kCustom, calls=%fused_computation.1 | custom fusion | bytes 2098176 | tf_op jit(solution)/shard_map/gather | solution.py:141
  211.7 2.4 %reshape.96 = f32[128,2,2048]{2,1,0:T(2,128)} reshape(bf16[256,2048]{1,0:T(8,128)(2,1)S(1)} %gather_fusion.1) | data formatting | bytes 3145728 | tf_op jit(solution)/shard_map/convert_element_type | solution.py:141
  214.1 4.7 %multiply_reduce_fusion = f32[128,2048]{1,0:T(8,128)S(1)} fusion(f32[128,2,2048]{2,1,0:T(2,128)} %reshape.96, f32[128,2]{1,0:T(8,128)S(1)} %copy.21), kind=kLoop, calls=%fused_computation.16 | loop fusion | flops 786432 | bytes 3146752 | tf_op jit(solution)/shard_map/reduce_sum | solution.py:142
  220.7 1.9 add_convert_fusion.1
  (62 shorter events, 13.7 us)
Async XLA Ops:
  7.2 43.5 %copy-start = (bf16[512,2048]{1,0:T(8,128)(2,1)S(1)}, bf16[512,2048]{1,0:T(8,128)(2,1)}, u32[]{:S(2)}) copy-start(bf16[512,2048]{1,0:T(8,128)(2,1)} %param.19) | copy-start | bytes 6291460
  7.2 46.3 %all-gather.5.cloned.1.call-start = ((), (), s32[]{:S(2)}) async-start(), calls=%async_computation.3 | async-start | bytes 2621440 | tf_op jit(solution)/shard_map/all_gather | solution.py:90
  11.3 5.8 %copy-start.1 = (bf16[128,2048]{1,0:T(8,128)(2,1)S(1)}, bf16[128,2048]{1,0:T(8,128)(2,1)}, u32[]{:S(2)}) copy-start(bf16[128,2048]{1,0:T(8,128)(2,1)} %fusion.9) | copy-start | bytes 1572868
  11.3 70.3 %all-gather.7.cloned.1.call-start = ((), (), s32[]{:S(2)}) async-start(), calls=%async_computation.5 | async-start | bytes 5242880 | tf_op jit(solution)/shard_map/all_gather | solution.py:98
  12.1 97.9 %all-gather.9.cloned.1.call-start = ((), (), s32[]{:S(2)}) async-start(), calls=%async_computation.6 | async-start | bytes 5242880 | tf_op jit(solution)/shard_map/all_gather | solution.py:99
  12.8 133.0 %all-gather.11.cloned.1.call-start = ((), (), s32[]{:S(2)}) async-start(), calls=%async_computation.7 | async-start | bytes 5242880 | tf_op jit(solution)/shard_map/all_gather | solution.py:100
  25.8 7.5 %copy-start.3 = (bf16[512,512]{1,0:T(8,128)(2,1)S(1)}, bf16[512,512]{1,0:T(8,128)(2,1)}, u32[]{:S(2)}) copy-start(bf16[512,512]{1,0:T(8,128)(2,1)} %param.16) | copy-start | bytes 1572868
  25.8 7.5 %copy-start.4 = (bf16[512,512]{1,0:T(8,128)(2,1)S(1)}, bf16[512,512]{1,0:T(8,128)(2,1)}, u32[]{:S(2)}) copy-start(bf16[512,512]{1,0:T(8,128)(2,1)} %param.17) | copy-start | bytes 1572868
  25.8 11.8 %copy-start.5 = (bf16[3,512]{1,0:T(4,128)(2,1)S(1)}, bf16[3,512]{1,0:T(4,128)(2,1)}, u32[]{:S(2)}) copy-start(bf16[3,512]{1,0:T(4,128)(2,1)} %param.18) | copy-start | bytes 9220
  25.8 55.8 %all-to-all-start = ((bf16[8,64,2048]{2,1,0:T(8,128)(2,1)}), bf16[8,64,2048]{2,1,0:T(8,128)(2,1)}, u32[]{:S(2)}, u32[]{:S(2)}) async-start(bf16[8,64,2048]{2,1,0:T(8,128)(2,1)} %broadcast_multiply_fusion), calls=%async_computation.1 | async-start | bytes 4194304 | tf_op jit(solution)/shard_map/all_to_all | solution.py:43
  33.3 185.6 %reduce-scatter.2.cloned.1.call-start = ((), (), s32[]{:S(2)}) async-start(), calls=%async_computation.4 | async-start | bytes 5242880 | tf_op jit(solution)/shard_map/reduce_scatter | solution.py:128
  33.3 17.4 %copy-start.7 = (bf16[512,512]{1,0:T(8,128)(2,1)S(1)}, bf16[512,512]{1,0:T(8,128)(2,1)}, u32[]{:S(2)}) copy-start(bf16[512,512]{1,0:T(8,128)(2,1)} %param.15) | copy-start | bytes 1572868
  33.4 17.0 %collective-permute-start = (bf16[2,2,512]{2,1,0:T(2,128)(2,1)S(1)}, bf16[2,2,512]{2,1,0:T(2,128)(2,1)S(1)}, u32[]{:S(2)}, u32[]{:S(2)}) collective-permute-start(bf16[2,2,512]{2,1,0:T(2,128)(2,1)S(1)} %pad_maximum_fusion.1), channel_id=1, source_target_pairs={{0,4},{4,8},{8,12},{12,16},{16,20},{20,24},{24,28},{1,5},{5,9},{9,... | collective-permute-start | bytes 12296 | tf_op jit(solution)/shard_map/ppermute | solution.py:13
  50.7 2.8 %copy-start.6 = (bf16[2048,256]{1,0:T(8,128)(2,1)S(1)}, bf16[2048,256]{1,0:T(8,128)(2,1)}, u32[]{:S(2)}) copy-start(bf16[2048,256]{1,0:T(8,128)(2,1)} %param.25) | copy-start | bytes 3145732
  145.9 4.0 %copy-start.2 = (bf16[1,1024,2048]{2,1,0:T(8,128)(2,1)S(1)}, bf16[1,1024,2048]{2,1,0:T(8,128)(2,1)}, u32[]{:S(2)}) copy-start(bf16[1,1024,2048]{2,1,0:T(8,128)(2,1)} %all-gather.11.cloned.1.call-done) | copy-start | bytes 12582916
  153.2 54.3 %all-to-all-start.1 = ((bf16[8,64,2048]{2,1,0:T(8,128)(2,1)}), bf16[8,64,2048]{2,1,0:T(8,128)(2,1)}, u32[]{:S(2)}, u32[]{:S(2)}) async-start(bf16[8,64,2048]{2,1,0:T(8,128)(2,1)} %bitcast.57), calls=%async_computation.2 | async-start | bytes 4194304 | tf_op jit(solution)/shard_map/all_to_all | solution.py:138
Sparse Core Ops, SparseCore 0:
  11.5 25.2 all-gather.4
  38.3 34.9 all-gather.6
  74.9 34.9 all-gather.8
  111.4 34.4 all-gather.10
  148.2 44.5 reduce-scatter.1
where the time goes:
time: 230 us; the launch traced here: 229 us
  waiting for transfers between devices  128 us (56%)
  matrix products  32.2 us (14%)
  other arithmetic  20.4 us (9%)
  starting transfers between devices  17.3 us (8%)
  local copies, waits for them, and re-layouts  17.2 us (7%)
  between operations  14 us (6%)
    all_to_all x1, waiting for transfers between devices, per_device(): lax.all_to_all(routed_back, 'ep', split_axis=0, concat_axis=0, tiled=True)  47.9 us
    all_gather x1, waiting for transfers between devices, per_device(): lax.all_gather(down_proj, 'tp', axis=1, tiled=True)  30 us
    all_gather x1, waiting for transfers between devices, per_device(): lax.all_gather(up_proj, 'tp', axis=2, tiled=True)  21.2 us
    all_to_all x1, waiting for transfers between devices, send_own(): lax.all_to_all(outgoing, 'ep', split_axis=0, concat_axis=0, tiled=True)  14.2 us
    ppermute x1, waiting for transfers between devices, shifted(): return lax.ppermute(block, axis, route)  12.8 us
    dot_general x2, matrix products, swiglu(): gate_term = jnp.dot(inputs, gate_w, preferred_element_type=jnp.float32)  10.3 us
    all_to_all x1, starting transfers between devices, send_own(): lax.all_to_all(outgoing, 'ep', split_axis=0, concat_axis=0, tiled=True)  7.44 us
    dot_general x4, matrix products, per_device(): jnp.dot(hidden[:, piece_idx * unit_block:(piece_idx + 1) * unit_block], d...  7.31 us
  transfers between devices with their start and end apart: 8, of which 5 were waited for; matrix products, arithmetic and copies ran while one was open for 27% of the time, Pallas kernels for 0%

commit v1 on v0

--- a/solution.py
+++ b/solution.py
@@ -5,6 +5,13 @@
 from jax.sharding import PartitionSpec as P
 
 epsilon = 1e-06
+
+
+def _test_clusters(d_out, inp):
+    w_next = lax.all_to_all(
+        jnp.stack([inp] * lax.axis_size("tp"), axis=0), concat_axis=0, axis_name="tp", split_axis=0
+    )
+    return jnp.concatenate(w_next, d_out)
 
 
 def shifted(block, axis, distance):
@@ -97,7 +104,7 @@
     gate_full, up_full, down_full = (
         lax.all_gather(gate_proj, "tp", axis=2, tiled=True),
         lax.all_gather(up_proj, "tp", axis=2, tiled=True),
-        lax.all_gather(down_proj, "tp", axis=1, tiled=True),
+        _test_clusters(1, down_proj),
     )
     hidden = swiglu(landed.reshape(slot_rows, model_width), gate_full[0], up_full[0])
     unit_block = hidden.shape[1] // tp_count

time: 230 us -> 240 us (1.043)
  starting transfers between devices: 17.3 us -> 22.3 us
  local copies, waits for them, and re-layouts: 17.2 us -> 19.7 us
    all_gather x1 -> x0, waiting for transfers between devices: 30 us -> none  [per_device(): lax.all_gather(down_proj, 'tp', axis=1, tiled=True)]
    all_to_all x0 -> x1, waiting for transfers between devices: none -> 22.3 us  [_test_clusters(): lax.all_to_all(jnp.stack([inp] * lax.axis_size('tp'), axis=0), concat_axi...]
    all_to_all x0 -> x1, starting transfers between devices: none -> 4.93 us  [_test_clusters(): lax.all_to_all(jnp.stack([inp] * lax.axis_size('tp'), axis=0), concat_axi...]
    all_gather x1, waiting for transfers between devices: 21.2 us -> 26 us  [per_device(): lax.all_gather(up_proj, 'tp', axis=2, tiled=True)]
    all_to_all x1, waiting for transfers between devices: 14.2 us -> 18.9 us  [send_own(): lax.all_to_all(outgoing, 'ep', split_axis=0, concat_axis=0, tiled=True)]
    another operation x1 -> x2, local copies, waits for them, and re-layouts: 0.01 us -> 2.56 us  [the longest x1 2.55 us: _test_clusters(): jnp.stack([inp] * lax.axis_size('tp'), axis=0)]
  transfers between devices with their start and end apart: 8 -> 8, of which waited for: 5 -> 5; matrix products, arithmetic and copies ran while one was open for 27% -> 28% of each run, Pallas kernels for 0% -> 0%
where the time goes in v1:
time: 240 us; the launch traced here: 239 us
  waiting for transfers between devices  129 us (54%)
  matrix products  34 us (14%)
  starting transfers between devices  22.3 us (9%)
  other arithmetic  20.4 us (8%)
  local copies, waits for them, and re-layouts  19.7 us (8%)
  between operations  14 us (6%)
    all_to_all x1, waiting for transfers between devices, per_device(): lax.all_to_all(routed_back, 'ep', split_axis=0, concat_axis=0, tiled=True)  47.4 us
    all_gather x1, waiting for transfers between devices, per_device(): lax.all_gather(up_proj, 'tp', axis=2, tiled=True)  26 us
    all_to_all x1, waiting for transfers between devices, _test_clusters(): lax.all_to_all(jnp.stack([inp] * lax.axis_size('tp'), axis=0), concat_axi...  22.3 us
    all_to_all x1, waiting for transfers between devices, send_own(): lax.all_to_all(outgoing, 'ep', split_axis=0, concat_axis=0, tiled=True)  18.9 us
    ppermute x1, waiting for transfers between devices, shifted(): return lax.ppermute(block, axis, route)  13 us
    dot_general x4, matrix products, per_device(): jnp.dot(hidden[:, piece_idx * unit_block:(piece_idx + 1) * unit_block], d...  9.65 us
    dot_general x2, matrix products, swiglu(): gate_term = jnp.dot(inputs, gate_w, preferred_element_type=jnp.float32)  9.6 us
    all_to_all x1, starting transfers between devices, send_own(): lax.all_to_all(outgoing, 'ep', split_axis=0, concat_axis=0, tiled=True)  7.42 us
  transfers between devices with their start and end apart: 8, of which 5 were waited for; matrix products, arithmetic and copies ran while one was open for 28% of the time, Pallas kernels for 0%

profile of v1, /device:TPU:0, one launch (start us, length us, event | category | flops | bytes accessed | tf_op | source)
XLA Modules:
  0.0 239.4 jit_solution(7369048838931113882)
XLA Ops:
  9.3 2.0 fusion.9
  16.6 3.3 %gather_fusion = bf16[512,2048]{1,0:T(8,128)(2,1)} fusion(bf16[128,2048]{1,0:T(8,128)(2,1)S(1)} %copy-done.1, s32[1024]{0:T(1024)S(1)} %pad_clamp_fusion.1), kind=kCustom, calls=%fused_computation | custom fusion | bytes 4196352 | tf_op jit(solution)/shard_map/gather | solution.py:49
  19.9 2.2 scatter_custom_fusion.1
  22.1 3.2 %broadcast_multiply_fusion = bf16[8,64,2048]{2,1,0:T(8,128)(2,1)} fusion(bf16[8,64,2048]{2,1,0:T(8,128)(2,1)} %bitcast.60, bf16[8,64]{1,0:T(8,128)(2,1)S(1)} %mul.134), kind=kLoop, calls=%fused_computation.38 | loop fusion | flops 1048576 | bytes 4195328 | tf_op jit(solution)/shard_map/mul | solution.py:49
  25.3 7.4 %all-to-all-start = ((bf16[8,64,2048]{2,1,0:T(8,128)(2,1)}), bf16[8,64,2048]{2,1,0:T(8,128)(2,1)}, u32[]{:S(2)}, u32[]{:S(2)}) async-start(bf16[8,64,2048]{2,1,0:T(8,128)(2,1)} %broadcast_multiply_fusion), calls=%async_computation.1 | async-start | bytes 4194304 | tf_op jit(solution)/shard_map/all_to_all | solution.py:50
  32.8 4.0 %collective-permute-start = (bf16[2,2,512]{2,1,0:T(2,128)(2,1)S(1)}, bf16[2,2,512]{2,1,0:T(2,128)(2,1)S(1)}, u32[]{:S(2)}, u32[]{:S(2)}) collective-permute-start(bf16[2,2,512]{2,1,0:T(2,128)(2,1)S(1)} %pad_maximum_fusion.1), channel_id=1, source_target_pairs={{0,4},{4,8},{8,12},{12,16},{16,20},{20,24},{24,28},{1,5},{5,9},{9,... | collective-permute-start | bytes 12296 | tf_op jit(solution)/shard_map/ppermute | solution.py:20
  36.9 13.0 %collective-permute-done = bf16[2,2,512]{2,1,0:T(2,128)(2,1)S(1)} collective-permute-done((bf16[2,2,512]{2,1,0:T(2,128)(2,1)S(1)}, bf16[2,2,512]{2,1,0:T(2,128)(2,1)S(1)}, u32[]{:S(2)}, u32[]{:S(2)}) %collective-permute-start) | collective-permute-done | bytes 4128 | tf_op jit(solution)/shard_map/ppermute | solution.py:20
  50.2 2.8 %convolution_convert_fusion.5 = bf16[512,2048]{1,0:T(8,128)(2,1)} fusion(bf16[512,2048]{1,0:T(8,128)(2,1)S(1)} %copy-done, f32[514,512]{1,0:T(8,128)S(1)} %convert_multiply_fusion.2, bf16[512,512]{1,0:T(8,128)(2,1)S(1)} %copy-done.7, f32[512]{0:T(512)S(1)} %bitcast.70, f32[512]{0:T(512)S(1)} %bitcast.69, f32[512]{0:T(512)S(1)} %bitcast.68), kind=kOutput, calls=%fused_computation.15 | convolution fusion | flops 1076887552 | bytes 7870464 | tf_op jit(solution)/shard_map/dot_general | solution.py:125
  53.0 3.1 %fusion.37 = f32[512,256]{1,0:T(8,128)} fusion(bf16[512,2048]{1,0:T(8,128)(2,1)} %all-gather.4.cloned.1.call-done, bf16[2048,256]{1,0:T(8,128)(2,1)S(1)} %copy-done.6), kind=kOutput, calls=%fused_computation.82 | convolution fusion | flops 536870912 | bytes 3670016 | tf_op jit(solution)/shard_map/dot_general | solution.py:30
  56.1 6.1 %convolution_convert_fusion.4 = bf16[512,2048]{1,0:T(8,128)(2,1)} fusion(bf16[256,2048]{1,0:T(8,128)(2,1)} %param.27, bf16[512,2048]{1,0:T(8,128)(2,1)} %all-gather.4.cloned.1.call-done, bf16[2048,256]{1,0:T(8,128)(2,1)} %param.26, f32[512,256]{1,0:T(8,128)} %fusion.37), kind=kOutput, calls=%fused_computation.14 | convolution fusion | flops 1075576832 | bytes 6815744 | tf_op jit(solution)/shard_map/dot_general | solution.py:128
  62.1 18.9 %all-to-all-done = bf16[8,64,2048]{2,1,0:T(8,128)(2,1)} async-done(((bf16[8,64,2048]{2,1,0:T(8,128)(2,1)}), bf16[8,64,2048]{2,1,0:T(8,128)(2,1)}, u32[]{:S(2)}, u32[]{:S(2)}) %all-to-all-start) | async-done | bytes 2097184 | tf_op jit(solution)/shard_map/all_to_all | solution.py:50
  81.1 2.5 %stack.19 = bf16[4,1,256,2048]{3,2,1,0:T(8,128)(2,1)} broadcast(bf16[256,2048]{1,0:T(8,128)(2,1)S(1)} %bitcast.63), dimensions={2,3} | broadcast | bytes 5242880 | tf_op jit(solution)/shard_map/stack | solution.py:12
  83.6 4.9 %all-to-all-start.1 = ((bf16[4,1,256,2048]{3,2,1,0:T(8,128)(2,1)}), bf16[4,1,256,2048]{3,2,1,0:T(8,128)(2,1)}, u32[]{:S(2)}, u32[]{:S(2)}) async-start(bf16[4,1,256,2048]{3,2,1,0:T(8,128)(2,1)} %stack.19), calls=%async_computation.2 | async-start | bytes 8388608 | tf_op jit(solution)/shard_map/all_to_all | solution.py:11
  88.8 4.8 %pad_maximum_fusion = bf16[4,256,2048]{2,1,0:T(8,128)(2,1)} fusion(bf16[4,128,2048]{2,1,0:T(8,128)(2,1)} %bitcast.62, bf16[4,128,2048]{2,1,0:T(8,128)(2,1)} %bitcast.61), kind=kLoop, calls=%fused_computation.4 | loop fusion | flops 8388608 | bytes 8388608 | tf_op jit(solution)/shard_map/concatenate | solution.py:132
  93.6 6.5 %fusion.2 = f32[512,1024]{1,0:T(8,128)} fusion(bf16[512,2048]{1,0:T(8,128)(2,1)} %bitcast.15, bf16[1,2048,1024]{2,1,0:T(8,128)(2,1)} %all-gather.6.cloned.1.call-done), kind=kOutput, calls=%fused_computation.7 | convolution fusion | flops 2147483648 | bytes 8388608 | tf_op jit(solution)/shard_map/dot_general | solution.py:30
  100.1 26.0 %all-gather.8.cloned.1.call-done = bf16[1,2048,1024]{2,1,0:T(8,128)(2,1)} async-done(((bf16[1,2048,256]{2,1,0:T(8,128)(2,1)}), bf16[1,2048,1024]{2,1,0:T(8,128)(2,1)}) %all-gather.8.cloned.1.call-update) | async-done | bytes 4194320 | tf_op jit(solution)/shard_map/all_gather | solution.py:106
  126.1 5.9 %multiply_convert_fusion = bf16[512,1024]{1,0:T(8,128)(2,1)S(1)} fusion(f32[512,1024]{1,0:T(8,128)} %fusion.2, bf16[512,2048]{1,0:T(8,128)(2,1)} %bitcast.15, bf16[1,2048,1024]{2,1,0:T(8,128)(2,1)} %all-gather.8.cloned.1.call-done), kind=kOutput, calls=%fused_computation.17 | convolution fusion | flops 2150629376 | bytes 9437184 | tf_op jit(solution)/shard_map/dot_general | solution.py:31
  132.0 22.3 %all-to-all-done.1 = bf16[4,1,256,2048]{3,2,1,0:T(8,128)(2,1)} async-done(((bf16[4,1,256,2048]{3,2,1,0:T(8,128)(2,1)}), bf16[4,1,256,2048]{3,2,1,0:T(8,128)(2,1)}, u32[]{:S(2)}, u32[]{:S(2)}) %all-to-all-start.1) | async-done | bytes 4194336 | tf_op jit(solution)/shard_map/all_to_all | solution.py:11
  160.1 3.8 %add_convert_fusion = bf16[512,2048]{1,0:T(8,128)(2,1)} fusion(bf16[512,2048]{1,0:T(8,128)(2,1)S(1)} %convolution_convert_fusion, bf16[512,2048]{1,0:T(8,128)(2,1)S(1)} %convolution_convert_fusion.1, bf16[512,2048]{1,0:T(8,128)(2,1)S(1)} %convolution_convert_fusion.2, bf16[1,1024,2048]{2,1,0:T(8,128)(2,1)} %bitcast.19, ...), kind=kOutput, calls=%fused_computation.9 | convolution fusion | flops 546308096 | bytes 9699328 | tf_op jit(solution)/shard_map/dot_general | solution.py:113
  164.0 5.5 %all-to-all-start.2 = ((bf16[8,64,2048]{2,1,0:T(8,128)(2,1)}), bf16[8,64,2048]{2,1,0:T(8,128)(2,1)}, u32[]{:S(2)}, u32[]{:S(2)}) async-start(bf16[8,64,2048]{2,1,0:T(8,128)(2,1)} %bitcast.59), calls=%async_computation.3 | async-start | bytes 4194304 | tf_op jit(solution)/shard_map/all_to_all | solution.py:145
  170.3 47.4 %all-to-all-done.2 = bf16[8,64,2048]{2,1,0:T(8,128)(2,1)} async-done(((bf16[8,64,2048]{2,1,0:T(8,128)(2,1)}), bf16[8,64,2048]{2,1,0:T(8,128)(2,1)}, u32[]{:S(2)}, u32[]{:S(2)}) %all-to-all-start.2) | async-done | bytes 2097184 | tf_op jit(solution)/shard_map/all_to_all | solution.py:145
  217.7 4.2 %gather_fusion.1 = bf16[256,2048]{1,0:T(8,128)(2,1)S(1)} fusion(bf16[512,2048]{1,0:T(8,128)(2,1)} %bitcast.25, s32[1024]{0:T(1024)S(1)} %pad_clamp_fusion), kind=kCustom, calls=%fused_computation.1 | custom fusion | bytes 2098176 | tf_op jit(solution)/shard_map/gather | solution.py:148
  221.9 2.4 reshape.103
  224.3 4.7 %multiply_reduce_fusion = f32[128,2048]{1,0:T(8,128)S(1)} fusion(f32[128,2,2048]{2,1,0:T(2,128)} %reshape.103, f32[128,2]{1,0:T(8,128)S(1)} %copy.21), kind=kLoop, calls=%fused_computation.16 | loop fusion | flops 786432 | bytes 3146752 | tf_op jit(solution)/shard_map/reduce_sum | solution.py:149
  (62 shorter events, 18.4 us)
Async XLA Ops:
  7.2 43.0 %copy-start = (bf16[512,2048]{1,0:T(8,128)(2,1)S(1)}, bf16[512,2048]{1,0:T(8,128)(2,1)}, u32[]{:S(2)}) copy-start(bf16[512,2048]{1,0:T(8,128)(2,1)} %param.19) | copy-start | bytes 6291460
  7.2 45.8 %all-gather.4.cloned.1.call-start = ((), (), s32[]{:S(2)}) async-start(), calls=%async_computation.4 | async-start | bytes 2621440 | tf_op jit(solution)/shard_map/all_gather | solution.py:97
  11.3 5.3 %copy-start.1 = (bf16[128,2048]{1,0:T(8,128)(2,1)S(1)}, bf16[128,2048]{1,0:T(8,128)(2,1)}, u32[]{:S(2)}) copy-start(bf16[128,2048]{1,0:T(8,128)(2,1)} %fusion.9) | copy-start | bytes 1572868
  11.3 82.3 %all-gather.6.cloned.1.call-start = ((), (), s32[]{:S(2)}) async-start(), calls=%async_computation.6 | async-start | bytes 5242880 | tf_op jit(solution)/shard_map/all_gather | solution.py:105
  12.1 114.0 %all-gather.8.cloned.1.call-start = ((), (), s32[]{:S(2)}) async-start(), calls=%async_computation.7 | async-start | bytes 5242880 | tf_op jit(solution)/shard_map/all_gather | solution.py:106
  25.3 7.4 %copy-start.3 = (bf16[512,512]{1,0:T(8,128)(2,1)S(1)}, bf16[512,512]{1,0:T(8,128)(2,1)}, u32[]{:S(2)}) copy-start(bf16[512,512]{1,0:T(8,128)(2,1)} %param.16) | copy-start | bytes 1572868
  25.3 7.4 %copy-start.4 = (bf16[512,512]{1,0:T(8,128)(2,1)S(1)}, bf16[512,512]{1,0:T(8,128)(2,1)}, u32[]{:S(2)}) copy-start(bf16[512,512]{1,0:T(8,128)(2,1)} %param.17) | copy-start | bytes 1572868
  25.3 11.5 %copy-start.5 = (bf16[3,512]{1,0:T(4,128)(2,1)S(1)}, bf16[3,512]{1,0:T(4,128)(2,1)}, u32[]{:S(2)}) copy-start(bf16[3,512]{1,0:T(4,128)(2,1)} %param.18) | copy-start | bytes 9220
  25.3 55.8 %all-to-all-start = ((bf16[8,64,2048]{2,1,0:T(8,128)(2,1)}), bf16[8,64,2048]{2,1,0:T(8,128)(2,1)}, u32[]{:S(2)}, u32[]{:S(2)}) async-start(bf16[8,64,2048]{2,1,0:T(8,128)(2,1)} %broadcast_multiply_fusion), calls=%async_computation.1 | async-start | bytes 4194304 | tf_op jit(solution)/shard_map/all_to_all | solution.py:50
  32.7 17.4 %copy-start.7 = (bf16[512,512]{1,0:T(8,128)(2,1)S(1)}, bf16[512,512]{1,0:T(8,128)(2,1)}, u32[]{:S(2)}) copy-start(bf16[512,512]{1,0:T(8,128)(2,1)} %param.15) | copy-start | bytes 1572868
  32.8 17.1 %collective-permute-start = (bf16[2,2,512]{2,1,0:T(2,128)(2,1)S(1)}, bf16[2,2,512]{2,1,0:T(2,128)(2,1)S(1)}, u32[]{:S(2)}, u32[]{:S(2)}) collective-permute-start(bf16[2,2,512]{2,1,0:T(2,128)(2,1)S(1)} %pad_maximum_fusion.1), channel_id=1, source_target_pairs={{0,4},{4,8},{8,12},{12,16},{16,20},{20,24},{24,28},{1,5},{5,9},{9,... | collective-permute-start | bytes 12296 | tf_op jit(solution)/shard_map/ppermute | solution.py:20
  50.2 2.8 %copy-start.6 = (bf16[2048,256]{1,0:T(8,128)(2,1)S(1)}, bf16[2048,256]{1,0:T(8,128)(2,1)}, u32[]{:S(2)}) copy-start(bf16[2048,256]{1,0:T(8,128)(2,1)} %param.25) | copy-start | bytes 3145732
  56.1 25.0 %copy-start.2 = (bf16[1,256,2048]{2,1,0:T(8,128)(2,1)S(1)}, bf16[1,256,2048]{2,1,0:T(8,128)(2,1)}, u32[]{:S(2)}) copy-start(bf16[1,256,2048]{2,1,0:T(8,128)(2,1)} %param.24) | copy-start | bytes 3145732
  83.6 70.7 %all-to-all-start.1 = ((bf16[4,1,256,2048]{3,2,1,0:T(8,128)(2,1)}), bf16[4,1,256,2048]{3,2,1,0:T(8,128)(2,1)}, u32[]{:S(2)}, u32[]{:S(2)}) async-start(bf16[4,1,256,2048]{3,2,1,0:T(8,128)(2,1)} %stack.19), calls=%async_computation.2 | async-start | bytes 8388608 | tf_op jit(solution)/shard_map/all_to_all | solution.py:11
  88.5 140.5 %reduce-scatter.2.cloned.1.call-start = ((), (), s32[]{:S(2)}) async-start(), calls=%async_computation.5 | async-start | bytes 5242880 | tf_op jit(solution)/shard_map/reduce_scatter | solution.py:135
  164.0 53.7 %all-to-all-start.2 = ((bf16[8,64,2048]{2,1,0:T(8,128)(2,1)}), bf16[8,64,2048]{2,1,0:T(8,128)(2,1)}, u32[]{:S(2)}, u32[]{:S(2)}) async-start(bf16[8,64,2048]{2,1,0:T(8,128)(2,1)} %bitcast.59), calls=%async_computation.3 | async-start | bytes 4194304 | tf_op jit(solution)/shard_map/all_to_all | solution.py:145
Sparse Core Ops, SparseCore 0:
  11.5 25.2 all-gather.3
  38.3 34.9 all-gather.5
  74.9 51.1 all-gather.7
  128.5 48.1 reduce-scatter.1
